TPU v7x, 32 devices: a whole 2x2x4 slice. The times are simulated.
32 devices in a mesh: ep: 16 (over z, x, core), tp: 2 (over y).
Axes of the slice: x: 2, y: 2, z: 4, core: 2. Of those that a mesh axis runs over, the one named last changes fastest.
Arguments:
- mix_input: bfloat16 [8192, 1024], P(('ep', 'tp')), may hold values from -6 to 6
- pool_weight: bfloat16 [8, 128, 128], replicated, may hold values from -0.5 to 0.5
- pool_scale: float32 [1024], replicated, may hold values from 0.1 to 1.9
- out_weight: bfloat16 [1024, 2048], replicated, may hold values from -0.1875 to 0.1875
- moe_input: bfloat16 [2048, 2048], P('ep'), may hold values from -6 to 6
- moe_gain: float32 [2048], replicated, may hold values from 0.1 to 1.9
- group_router: bfloat16 [2048, 4], replicated, may hold values from -0.125 to 0.125
- inner_router: bfloat16 [2048, 16], replicated, may hold values from -0.125 to 0.125
- group_pick: int32 [2048], P('ep'), may hold values from 0 to 3
- inner_pick: int32 [2048, 2], P('ep'), may hold values from 0 to 3, all different within a row
- gate_weight: bfloat16 [16, 2048, 1024], P('ep', None, 'tp'), may hold values from -0.125 to 0.125
- up_weight: bfloat16 [16, 2048, 1024], P('ep', None, 'tp'), may hold values from -0.125 to 0.125
- down_weight: bfloat16 [16, 1024, 2048], P('ep', 'tp'), may hold values from -0.1875 to 0.1875
Outputs:
- mix_out: bfloat16 [8192, 2048], P(('ep', 'tp'))
- moe_out: bfloat16 [2048, 2048], P('ep', 'tp')
All inputs are finite; a program needn't handle non-finite values.
Results may differ from a plain program's by a relative error of at most 0.011.
Values may be sent and summed in bfloat16 or wider, within the bound.
No kernel may reach another device: no remote copies, remote signals or barrier semaphores. Data moves between devices by JAX's collectives and lax.ppermute only.
A program may use at most 64 MiB of HBM per device.

v0:
```python
import jax
import jax.numpy as jnp
from jax import lax
from jax.sharding import PartitionSpec as P

WINDOW_MAX = 16
NORM_FLOOR = 0.25


def passed_along(value, axis, steps):
    count = lax.axis_size(axis)
    first, last = (max(0, -steps), min(count, count - steps))
    return lax.ppermute(value, axis, [(source, source + steps) for source in range(first, last)])


def trailing_means(extended, row_count, lead_rows, first_position):
    group_width = extended.shape[1] // 4
    position = first_position + jnp.arange(row_count, dtype=jnp.int32)
    pieces = []
    for scale_index in range(4):
        window = 2 ** (scale_index + 1)
        channel_block = extended[:, scale_index * group_width : (scale_index + 1) * group_width]
        window_sum = channel_block[lead_rows : lead_rows + row_count]
        for back_step in range(1, window):
            window_sum = (
                window_sum
                + channel_block[lead_rows - back_step : lead_rows - back_step + row_count]
            )
        divisor = jnp.minimum(position + 1, window).astype(jnp.float32)
        pieces.append(window_sum / divisor[:, None])
    return jnp.concatenate(pieces, axis=1)


def route_terms(group_logits, inner_logits, group_pick, inner_pick, per_group):
    group_ids = jnp.arange(group_logits.shape[1], dtype=jnp.int32)
    chosen = jnp.sum(
        jnp.where(group_pick[:, None] == group_ids[None, :], group_logits, 0.0), axis=1
    )
    group_share = 1.0 / jnp.sum(jnp.exp(group_logits - chosen[:, None]), axis=1)
    target = group_pick[:, None] * per_group + inner_pick
    expert_ids = jnp.arange(inner_logits.shape[1], dtype=jnp.int32)
    picked = jnp.sum(
        jnp.where(target[:, :, None] == expert_ids[None, None, :], inner_logits[:, None, :], 0.0),
        axis=2,
    )
    first_share = jax.nn.sigmoid(picked[:, 0] - picked[:, 1])
    route_weight = group_share[:, None] * jnp.stack([first_share, 1.0 - first_share], axis=1)
    return (target, route_weight)


def slot_terms(target, expert_count, capacity):
    expert_ids = jnp.arange(expert_count, dtype=jnp.int32)
    expert_hits = (target[:, :, None] == expert_ids[None, None, :]).astype(jnp.int32)
    per_token = jnp.sum(expert_hits, axis=1)
    earlier = jnp.cumsum(per_token, axis=0) - per_token
    route_rank = jnp.sum(expert_hits * earlier[:, None, :], axis=2)
    is_kept = route_rank < capacity
    slot_index = target * capacity + jnp.minimum(route_rank, capacity - 1)
    return (slot_index, is_kept)


def slot_sources(slot_index, is_kept, slot_count):
    token_ids = jnp.broadcast_to(
        jnp.arange(slot_index.shape[0], dtype=jnp.int32)[:, None], slot_index.shape
    )
    placed = jnp.where(is_kept, slot_index, slot_count).reshape(-1)
    source = jnp.zeros((slot_count,), jnp.int32).at[placed].set(token_ids.reshape(-1), mode="drop")
    slot_used = jnp.zeros((slot_count,), jnp.bool_).at[placed].set(True, mode="drop")
    return (source, slot_used)


def per_device(
    mix_input,
    pool_weight,
    pool_scale,
    out_weight,
    moe_input,
    moe_gain,
    group_router,
    inner_router,
    group_pick,
    inner_pick,
    gate_weight,
    up_weight,
    down_weight,
):
    row_count = mix_input.shape[0]
    reach_back = WINDOW_MAX - 1
    before = passed_along(mix_input[row_count - reach_back :], ("ep", "tp"), 1)
    extended = jnp.concatenate([before, mix_input], axis=0).astype(jnp.float32)
    first_position = lax.axis_index(("ep", "tp")) * row_count
    trailing = (
        trailing_means(extended, row_count, reach_back, first_position) - extended[reach_back:]
    )
    pooled = trailing.astype(jnp.bfloat16)
    groups, group_dim = (pool_weight.shape[0], pool_weight.shape[1])
    grouped = jnp.einsum(
        "tgc,gcd->tgd",
        pooled.reshape(row_count, groups, group_dim),
        pool_weight,
        preferred_element_type=jnp.float32,
    )
    grouped = (grouped.reshape(row_count, groups * group_dim) * pool_scale[None, :]).astype(
        jnp.bfloat16
    )
    mix_out = jnp.dot(grouped, out_weight, preferred_element_type=jnp.float32).astype(jnp.bfloat16)
    tokens, feature_width = moe_input.shape
    token_values = moe_input.astype(jnp.float32)
    norm_scale = lax.rsqrt(
        jnp.maximum(jnp.mean(token_values * token_values, axis=1, keepdims=True), NORM_FLOOR)
    )
    normed = (token_values * norm_scale * moe_gain[None, :]).astype(jnp.bfloat16)
    group_logits = jnp.dot(normed, group_router, preferred_element_type=jnp.float32)
    inner_logits = jnp.dot(normed, inner_router, preferred_element_type=jnp.float32)
    group_count = group_router.shape[1]
    expert_count = inner_router.shape[1]
    target, route_weight = route_terms(
        group_logits, inner_logits, group_pick, inner_pick, expert_count // group_count
    )
    capacity = 2 * inner_pick.shape[1] * tokens // expert_count
    slot_index, is_kept = slot_terms(target, expert_count, capacity)
    source, slot_used = slot_sources(slot_index, is_kept, expert_count * capacity)
    gate_local = gate_weight[0]
    up_local = up_weight[0]
    outgoing = jnp.where(slot_used[:, None], normed[source], jnp.zeros((), jnp.bfloat16))
    arrived = lax.all_to_all(outgoing, "ep", split_axis=0, concat_axis=0, tiled=True)
    gate_sum = jnp.dot(arrived, gate_local, preferred_element_type=jnp.float32)
    up_sum = jnp.dot(arrived, up_local, preferred_element_type=jnp.float32)
    hidden = (jax.nn.silu(gate_sum) * up_sum).astype(jnp.bfloat16)
    down_local = down_weight[0]
    expert_result = lax.psum_scatter(
        lax.dot_general(
            down_local, hidden, (((0,), (1,)), ((), ())), preferred_element_type=jnp.float32
        ).astype(jnp.bfloat16),
        "tp",
        scatter_dimension=0,
        tiled=True,
    )
    returned = lax.all_to_all(expert_result, "ep", split_axis=1, concat_axis=1, tiled=True)
    route_scale = jnp.where(is_kept, route_weight, 0.0).astype(jnp.bfloat16)
    route_scale = lax.optimization_barrier(route_scale).astype(jnp.float32)
    picked = jnp.take(returned, slot_index, axis=1).astype(jnp.float32)
    combined = jnp.sum(picked * route_scale[None, :, :], axis=2)
    moe_out = combined.T.astype(jnp.bfloat16)
    return (mix_out, moe_out)


def solution(mesh):
    in_specs = (
        P(("ep", "tp"), None),
        P(),
        P(),
        P(),
        P("ep", None),
        P(),
        P(),
        P(),
        P("ep"),
        P("ep", None),
        P("ep", None, "tp"),
        P("ep", None, "tp"),
        P("ep", "tp", None),
    )
    out_specs = (P(("ep", "tp"), None), P("ep", "tp"))
    return jax.shard_map(
        per_device, mesh=mesh, in_specs=in_specs, out_specs=out_specs, check_vma=False
    )
```

profile of v0, /device:TPU:9, one launch (start us, length us, event | category | flops | bytes accessed | tf_op | source)
XLA Modules:
  0.0 159.9 jit_solution(5411471820745294769)
XLA Ops:
  7.2 0.8 broadcast_multiply_fusion
  8.0 0.7 broadcast_add_fusion
  9.1 0.7 broadcast_select_fusion.2
  10.2 1.4 scatter_custom_fusion.1
  11.6 1.2 fusion.12
  12.9 1.5 scatter_custom_fusion
  14.5 1.2 fusion.14
  15.7 3.3 %gather_fusion = bf16[512,2048]{1,0:T(8,128)(2,1)} fusion(bf16[128,2048]{1,0:T(8,128)(2,1)S(1)} %fusion.14, s32[1024]{0:T(1024)S(1)} %pad_clamp_fusion.1), kind=kCustom, calls=%fused_computation | custom fusion | bytes 4196352 | tf_op jit(solution)/shard_map/gather | solution.py:125
  19.1 1.8 %broadcast_select_fusion = bf16[16,32,2048]{2,1,0:T(8,128)(2,1)S(1)} fusion(bf16[16,32,2048]{2,1,0:T(8,128)(2,1)} %bitcast.45, pred[16,32]{1,0:T(8,128)(4,1)S(1)} %broadcast_in_dim.88), kind=kLoop, calls=%fused_computation.12 | loop fusion | flops 1048576 | bytes 4194816 | tf_op jit(solution)/shard_map/jit(_where)/select_n | solution.py:125
  20.9 54.3 %all_to_all.21 = bf16[16,32,2048]{2,1,0:T(8,128)(2,1)S(1)} all-to-all(bf16[16,32,2048]{2,1,0:T(8,128)(2,1)S(1)} %broadcast_select_fusion), channel_id=1, replica_groups=mesh['ep'=16,'tp'=2] {'ep'}, dimensions={0} | all-to-all | bytes 4194304 | tf_op jit(solution)/shard_map/all_to_all | solution.py:126
  75.2 1.3 copy-done.1
  76.5 2.2 %fusion.4 = f32[512,512]{1,0:T(8,128)} fusion(bf16[512,2048]{1,0:T(8,128)(2,1)S(1)} %bitcast.46, bf16[1,2048,512]{2,1,0:T(8,128)(2,1)S(1)} %copy-done.8), kind=kOutput, calls=%fused_computation.10 | convolution fusion | flops 1073741824 | bytes 5242880 | tf_op jit(solution)/shard_map/dot_general | solution.py:127
  78.7 6.3 %fusion = bf16[2048,512]{0,1:T(8,128)(2,1)} fusion(bf16[1,512,2048]{2,1,0:T(8,128)(2,1)S(1)} %copy-done, bf16[512,2048]{1,0:T(8,128)(2,1)} %bitcast.47, bf16[1,2048,512]{2,1,0:T(8,128)(2,1)} %param.24, f32[512,512]{1,0:T(8,128)} %fusion.4), kind=kOutput, calls=%fused_computation.5 | convolution fusion | flops 2150105088 | bytes 9437184 | tf_op jit(solution)/shard_map/dot_general | solution.py:132
  85.0 0.8 slice.136
  85.8 3.1 %collective-permute-start = (bf16[15,1024]{1,0:T(8,128)(2,1)S(1)}, bf16[15,1024]{1,0:T(8,128)(2,1)S(1)}, u32[]{:S(2)}, u32[]{:S(2)}) collective-permute-start(bf16[15,1024]{1,0:T(8,128)(2,1)S(1)} %slice.136), channel_id=1, source_target_pairs={{0,1},{1,2},{2,3},{3,4},{4,5},{5,6},{6,7},{7,8},{8,9},{9,10},{10,1... | collective-permute-start | bytes 92168 | tf_op jit(solution)/shard_map/ppermute | solution.py:13
  89.0 0.3 select_reduce_fusion.2
  89.3 0.2 fusion.35
  89.6 26.4 %reduce-scatter.2.cloned.1.call-done = bf16[1024,512]{0,1:T(8,128)(2,1)} async-done(((bf16[2048,512]{0,1:T(8,128)(2,1)}), bf16[1024,512]{0,1:T(8,128)(2,1)}) %reduce-scatter.2.cloned.1.call-update) | async-done | bytes 1048592 | tf_op jit(solution)/shard_map/reduce_scatter | solution.py:131
  116.0 6.5 %all-to-all-start.1 = ((bf16[1024,16,32]{0,2,1:T(8,128)(2,1)}), bf16[1024,16,32]{0,2,1:T(8,128)(2,1)S(1)}, u32[]{:S(2)}, u32[]{:S(2)}) async-start(bf16[1024,16,32]{0,2,1:T(8,128)(2,1)} %bitcast.48), calls=%async_computation.2 | async-start | bytes 2097152 | tf_op jit(solution)/shard_map/all_to_all | solution.py:139
  123.1 1.2 maximum_convert_fusion
  124.3 0.3 fusion.24
  124.6 0.4 fusion.27
  125.0 0.6 copy-done.9
  125.6 0.3 fusion.19
  125.9 0.3 copy-done.5
  126.3 0.2 fusion.16
  126.5 1.3 copy-done.7
  127.8 2.2 %convolution_convert_fusion.1 = bf16[256,2048]{1,0:T(8,128)(2,1)} fusion(bf16[256,1024]{0,1:T(8,128)(2,1)S(1)} %fusion.16, bf16[1024,2048]{1,0:T(8,128)(2,1)S(1)} %copy-done.7), kind=kOutput, calls=%fused_computation.6 | convolution fusion | flops 1074266112 | bytes 5767168 | tf_op jit(solution)/shard_map/dot_general | solution.py:106
  130.0 17.4 %all-to-all-done.1 = bf16[1024,16,32]{0,2,1:T(8,128)(2,1)S(1)} async-done(((bf16[1024,16,32]{0,2,1:T(8,128)(2,1)}), bf16[1024,16,32]{0,2,1:T(8,128)(2,1)S(1)}, u32[]{:S(2)}, u32[]{:S(2)}) %all-to-all-start.1) | async-done | bytes 1048608 | tf_op jit(solution)/shard_map/all_to_all | solution.py:139
  147.5 2.0 %gather_fusion.1 = bf16[256,1024]{1,0:T(8,128)(2,1)} fusion(bf16[1024,512]{0,1:T(8,128)(2,1)S(1)} %bitcast.44, s32[1024]{0:T(1024)S(1)} %pad_clamp_fusion), kind=kCustom, calls=%fused_computation.1 | custom fusion | bytes 1049600 | tf_op jit(solution)/shard_map/jit(_take)/gather | solution.py:142
  149.4 1.2 reshape.125
  150.7 2.3 %multiply_reduce_fusion = bf16[128,1024]{1,0:T(8,128)(2,1)} fusion(bf16[128,2,1024]{2,1,0:T(2,128)(2,1)S(1)} %reshape.125, pred[128,2]{1,0:T(8,128)(4,1)S(1)} %copy.34, f32[128,2]{1,0:T(8,128)S(1)} %copy.37), kind=kLoop, calls=%fused_computation.24 | loop fusion | flops 917504 | bytes 787712 | tf_op jit(solution)/shard_map/reduce_sum | solution.py:143
  (48 shorter events, 1.6 us)
Async XLA Ops:
  7.2 71.5 %copy-start = (bf16[1,512,2048]{2,1,0:T(8,128)(2,1)S(1)}, bf16[1,512,2048]{2,1,0:T(8,128)(2,1)}, u32[]{:S(2)}) copy-start(bf16[1,512,2048]{2,1,0:T(8,128)(2,1)} %param.25) | copy-start | bytes 6291460
  7.2 108.8 %reduce-scatter.2.cloned.1.call-start = ((), (), s32[]{:S(2)}) async-start(), calls=%async_computation.3 | async-start | bytes 3145728 | tf_op jit(solution)/shard_map/reduce_scatter | solution.py:131
  20.9 55.6 %copy-start.8 = (bf16[1,2048,512]{2,1,0:T(8,128)(2,1)S(1)}, bf16[1,2048,512]{2,1,0:T(8,128)(2,1)}, u32[]{:S(2)}) copy-start(bf16[1,2048,512]{2,1,0:T(8,128)(2,1)} %param.23) | copy-start | bytes 6291460
  75.2 1.3 copy-start.1
  85.0 4.0 %copy-start.3 = (bf16[2048,4]{0,1:T(4,128)(2,1)S(1)}, bf16[2048,4]{0,1:T(4,128)(2,1)}, u32[]{:S(2)}) copy-start(bf16[2048,4]{0,1:T(4,128)(2,1)} %param.19) | copy-start | bytes 49156
  85.0 4.0 %copy-start.6 = (s32[128]{0:T(128)S(1)}, s32[128]{0:T(128)}, u32[]{:S(2)}) copy-start(s32[128]{0:T(128)} %param.21) | copy-start | bytes 1540
  85.0 4.3 %copy-start.2 = (bf16[2048,16]{0,1:T(8,128)(2,1)S(1)}, bf16[2048,16]{0,1:T(8,128)(2,1)}, u32[]{:S(2)}) copy-start(bf16[2048,16]{0,1:T(8,128)(2,1)} %param.20) | copy-start | bytes 196612
  85.0 4.6 %copy-start.4 = (s32[128,2]{0,1:T(2,128)S(1)}, s32[128,2]{0,1:T(2,128)}, u32[]{:S(2)}) copy-start(s32[128,2]{0,1:T(2,128)} %param.22) | copy-start | bytes 3076
  85.8 37.3 %collective-permute-start = (bf16[15,1024]{1,0:T(8,128)(2,1)S(1)}, bf16[15,1024]{1,0:T(8,128)(2,1)S(1)}, u32[]{:S(2)}, u32[]{:S(2)}) collective-permute-start(bf16[15,1024]{1,0:T(8,128)(2,1)S(1)} %slice.136), channel_id=1, source_target_pairs={{0,1},{1,2},{2,3},{3,4},{4,5},{5,6},{6,7},{7,8},{8,9},{9,10},{10,1... | collective-permute-start | bytes 92168 | tf_op jit(solution)/shard_map/ppermute | solution.py:13
  116.0 31.4 %all-to-all-start.1 = ((bf16[1024,16,32]{0,2,1:T(8,128)(2,1)}), bf16[1024,16,32]{0,2,1:T(8,128)(2,1)S(1)}, u32[]{:S(2)}, u32[]{:S(2)}) async-start(bf16[1024,16,32]{0,2,1:T(8,128)(2,1)} %bitcast.48), calls=%async_computation.2 | async-start | bytes 2097152 | tf_op jit(solution)/shard_map/all_to_all | solution.py:139
  124.6 1.0 copy-start.9
  125.6 0.7 copy-start.5
  125.6 2.2 %copy-start.7 = (bf16[1024,2048]{1,0:T(8,128)(2,1)S(1)}, bf16[1024,2048]{1,0:T(8,128)(2,1)}, u32[]{:S(2)}) copy-start(bf16[1024,2048]{1,0:T(8,128)(2,1)} %param.16) | copy-start | bytes 12582916
Sparse Core Ops, SparseCore 0:
  85.1 30.8 reduce-scatter.1
where the time goes:
time: 160 us
  blocking collectives  54.3 us (34%)
  waiting for transfers between devices  43.8 us (27%)
  local copies, waits for them, and re-layouts  14.9 us (9%)
  between operations  14.3 us (9%)
  matrix products  11.6 us (7%)
  other arithmetic  11.2 us (7%)
  starting transfers between devices  9.71 us (6%)
    all_to_all x1, blocking collectives, per_device(): lax.all_to_all(outgoing, 'ep', split_axis=0, concat_axis=0, tiled=True)  54.3 us
    reduce_scatter x1, waiting for transfers between devices, per_device(): lax.psum_scatter(lax.dot_general(down_local, hidden, (((0,), (1,)), ((),...  26.4 us
    all_to_all x1, waiting for transfers between devices, per_device(): lax.all_to_all(expert_result, 'ep', split_axis=1, concat_axis=1, tiled=True)  17.4 us
    all_to_all x1, starting transfers between devices, per_device(): lax.all_to_all(expert_result, 'ep', split_axis=1, concat_axis=1, tiled=True)  6.52 us
    dot_general x1, matrix products, per_device(): lax.dot_general(down_local, hidden, (((0,), (1,)), ((), ())), preferred_e...  6.27 us
    unnamed x20, local copies, waits for them, and re-layouts  3.54 us
    gather x1, local copies, waits for them, and re-layouts, per_device(): normed[source]  3.35 us
  transfers between devices with their start and end apart: 3, of which 2 were waited for; matrix products, arithmetic and copies ran while one was open for 4% of the time, Pallas kernels for 0%

commit v1 on v0

--- a/solution.py
+++ b/solution.py
@@ -136,7 +136,12 @@
         scatter_dimension=0,
         tiled=True,
     )
-    returned = lax.all_to_all(expert_result, "ep", split_axis=1, concat_axis=1, tiled=True)
+    returned = jnp.concatenate(
+        lax.all_to_all(
+            jnp.stack(jnp.split(expert_result, lax.axis_size("ep"), axis=1)), "ep", 0, 0
+        ),
+        axis=1,
+    )
     route_scale = jnp.where(is_kept, route_weight, 0.0).astype(jnp.bfloat16)
     route_scale = lax.optimization_barrier(route_scale).astype(jnp.float32)
     picked = jnp.take(returned, slot_index, axis=1).astype(jnp.float32)

time: 160 us -> 185 us (1.16)
  local copies, waits for them, and re-layouts: 14.9 us -> 38.3 us
    unnamed x20 -> x35, local copies, waits for them, and re-layouts: 3.54 us -> 25.5 us
  transfers between devices with their start and end apart: 3 -> 3, of which waited for: 2 -> 2; matrix products, arithmetic and copies ran while one was open for 4% -> 16% of each run, Pallas kernels for 0% -> 0%
where the time goes in v1:
time: 185 us; the launch traced here: 183 us
  blocking collectives  54.3 us (29%)
  waiting for transfers between devices  43.8 us (24%)
  local copies, waits for them, and re-layouts  38.3 us (21%)
  between operations  14.3 us (8%)
  matrix products  11.6 us (6%)
  other arithmetic  11.2 us (6%)
  starting transfers between devices  9.71 us (5%)
    all_to_all x1, blocking collectives, per_device(): lax.all_to_all(outgoing, 'ep', split_axis=0, concat_axis=0, tiled=True)  54.3 us
    reduce_scatter x1, waiting for transfers between devices, per_device(): lax.psum_scatter(lax.dot_general(down_local, hidden, (((0,), (1,)), ((),...  26.4 us
    unnamed x35, local copies, waits for them, and re-layouts  25.5 us
    all_to_all x1, waiting for transfers between devices, per_device(): lax.all_to_all(jnp.stack(jnp.split(expert_result, lax.axis_size('ep'), ax...  17.4 us
    all_to_all x1, starting transfers between devices, per_device(): lax.all_to_all(jnp.stack(jnp.split(expert_result, lax.axis_size('ep'), ax...  6.52 us
    dot_general x1, matrix products, per_device(): lax.dot_general(down_local, hidden, (((0,), (1,)), ((), ())), preferred_e...  6.27 us
  transfers between devices with their start and end apart: 3, of which 2 were waited for; matrix products, arithmetic and copies ran while one was open for 16% of the time, Pallas kernels for 0%

profile of v1, /device:TPU:9, one launch (start us, length us, event | category | flops | bytes accessed | tf_op | source)
XLA Modules:
  0.0 183.3 jit_solution(4304560074707034400)
XLA Ops:
  10.2 1.4 scatter_custom_fusion.1
  12.9 1.5 scatter_custom_fusion
  15.7 3.3 %gather_fusion = bf16[512,2048]{1,0:T(8,128)(2,1)} fusion(bf16[128,2048]{1,0:T(8,128)(2,1)S(1)} %fusion.14, s32[1024]{0:T(1024)S(1)} %pad_clamp_fusion.1), kind=kCustom, calls=%fused_computation | custom fusion | bytes 4196352 | tf_op jit(solution)/shard_map/gather | solution.py:125
  19.1 1.8 broadcast_select_fusion
  20.9 54.3 %all_to_all.14 = bf16[16,32,2048]{2,1,0:T(8,128)(2,1)S(1)} all-to-all(bf16[16,32,2048]{2,1,0:T(8,128)(2,1)S(1)} %broadcast_select_fusion), channel_id=1, replica_groups=mesh['ep'=16,'tp'=2] {'ep'}, dimensions={0} | all-to-all | bytes 4194304 | tf_op jit(solution)/shard_map/all_to_all | solution.py:126
  75.2 1.3 copy-done.1
  76.5 2.2 %fusion.4 = f32[512,512]{1,0:T(8,128)} fusion(bf16[512,2048]{1,0:T(8,128)(2,1)S(1)} %bitcast.111, bf16[1,2048,512]{2,1,0:T(8,128)(2,1)S(1)} %copy-done.8), kind=kOutput, calls=%fused_computation.10 | convolution fusion | flops 1073741824 | bytes 5242880 | tf_op jit(solution)/shard_map/dot_general | solution.py:127
  78.7 6.3 %fusion = bf16[2048,512]{0,1:T(8,128)(2,1)} fusion(bf16[1,512,2048]{2,1,0:T(8,128)(2,1)S(1)} %copy-done, bf16[512,2048]{1,0:T(8,128)(2,1)} %bitcast.112, bf16[1,2048,512]{2,1,0:T(8,128)(2,1)} %param.24, f32[512,512]{1,0:T(8,128)} %fusion.4), kind=kOutput, calls=%fused_computation.5 | convolution fusion | flops 2150105088 | bytes 9437184 | tf_op jit(solution)/shard_map/dot_general | solution.py:132
  85.8 3.1 %collective-permute-start = (bf16[15,1024]{1,0:T(8,128)(2,1)S(1)}, bf16[15,1024]{1,0:T(8,128)(2,1)S(1)}, u32[]{:S(2)}, u32[]{:S(2)}) collective-permute-start(bf16[15,1024]{1,0:T(8,128)(2,1)S(1)} %slice.136), channel_id=1, source_target_pairs={{0,1},{1,2},{2,3},{3,4},{4,5},{5,6},{6,7},{7,8},{8,9},{9,10},{10,1... | collective-permute-start | bytes 92168 | tf_op jit(solution)/shard_map/ppermute | solution.py:13
  89.6 26.4 %reduce-scatter.2.cloned.1.call-done = bf16[1024,512]{0,1:T(8,128)(2,1)} async-done(((bf16[2048,512]{0,1:T(8,128)(2,1)}), bf16[1024,512]{0,1:T(8,128)(2,1)}) %reduce-scatter.2.cloned.1.call-update) | async-done | bytes 1048592 | tf_op jit(solution)/shard_map/reduce_scatter | solution.py:131
  116.0 1.5 fusion.43
  117.5 1.5 fusion.42
  118.9 1.5 fusion.41
  120.4 1.5 fusion.40
  121.9 1.5 fusion.39
  123.3 1.5 fusion.38
  124.8 1.5 fusion.37
  126.3 1.5 fusion.36
  127.7 1.5 fusion.35
  129.2 1.5 fusion.34
  130.6 1.5 fusion.33
  132.1 1.5 fusion.32
  133.6 1.5 fusion.31
  135.0 1.5 fusion.30
  136.5 1.5 fusion.29
  137.9 1.5 fusion.28
  139.4 6.5 %all-to-all-start.1 = ((bf16[16,1024,32]{1,2,0:T(8,128)(2,1)}), bf16[16,1024,32]{1,2,0:T(8,128)(2,1)S(1)}, u32[]{:S(2)}, u32[]{:S(2)}) async-start(bf16[16,1024,32]{1,2,0:T(8,128)(2,1)} %fusion.28), calls=%async_computation.2 | async-start | bytes 2097152 | tf_op jit(solution)/shard_map/all_to_all | solution.py:140
  149.9 1.3 copy-done.7
  151.2 2.2 %convolution_convert_fusion.1 = bf16[256,2048]{1,0:T(8,128)(2,1)} fusion(bf16[256,1024]{0,1:T(8,128)(2,1)S(1)} %fusion.16, bf16[1024,2048]{1,0:T(8,128)(2,1)S(1)} %copy-done.7), kind=kOutput, calls=%fused_computation.6 | convolution fusion | flops 1074266112 | bytes 5767168 | tf_op jit(solution)/shard_map/dot_general | solution.py:106
  153.4 17.4 %all-to-all-done.1 = bf16[16,1024,32]{1,2,0:T(8,128)(2,1)S(1)} async-done(((bf16[16,1024,32]{1,2,0:T(8,128)(2,1)}), bf16[16,1024,32]{1,2,0:T(8,128)(2,1)S(1)}, u32[]{:S(2)}, u32[]{:S(2)}) %all-to-all-start.1) | async-done | bytes 1048608 | tf_op jit(solution)/shard_map/all_to_all | solution.py:140
  170.9 2.0 %gather_fusion.1 = bf16[256,1024]{1,0:T(8,128)(2,1)} fusion(bf16[1024,512]{0,1:T(8,128)(2,1)S(1)} %bitcast.109, s32[1024]{0:T(1024)S(1)} %pad_clamp_fusion), kind=kCustom, calls=%fused_computation.1 | custom fusion | bytes 1049600 | tf_op jit(solution)/shard_map/jit(_take)/gather | solution.py:147
  174.1 2.3 %multiply_reduce_fusion = bf16[128,1024]{1,0:T(8,128)(2,1)} fusion(bf16[128,2,1024]{2,1,0:T(2,128)(2,1)S(1)} %reshape.131, pred[128,2]{1,0:T(8,128)(4,1)S(1)} %copy.34, f32[128,2]{1,0:T(8,128)S(1)} %copy.37), kind=kLoop, calls=%fused_computation.24 | loop fusion | flops 917504 | bytes 787712 | tf_op jit(solution)/shard_map/reduce_sum | solution.py:148
  (64 shorter events, 12.1 us)
Async XLA Ops:
  7.2 71.5 %copy-start = (bf16[1,512,2048]{2,1,0:T(8,128)(2,1)S(1)}, bf16[1,512,2048]{2,1,0:T(8,128)(2,1)}, u32[]{:S(2)}) copy-start(bf16[1,512,2048]{2,1,0:T(8,128)(2,1)} %param.25) | copy-start | bytes 6291460
  7.2 108.8 %reduce-scatter.2.cloned.1.call-start = ((), (), s32[]{:S(2)}) async-start(), calls=%async_computation.3 | async-start | bytes 3145728 | tf_op jit(solution)/shard_map/reduce_scatter | solution.py:131
  20.9 55.6 %copy-start.8 = (bf16[1,2048,512]{2,1,0:T(8,128)(2,1)S(1)}, bf16[1,2048,512]{2,1,0:T(8,128)(2,1)}, u32[]{:S(2)}) copy-start(bf16[1,2048,512]{2,1,0:T(8,128)(2,1)} %param.23) | copy-start | bytes 6291460
  75.2 1.3 copy-start.1
  85.0 4.0 %copy-start.3 = (bf16[2048,4]{0,1:T(4,128)(2,1)S(1)}, bf16[2048,4]{0,1:T(4,128)(2,1)}, u32[]{:S(2)}) copy-start(bf16[2048,4]{0,1:T(4,128)(2,1)} %param.19) | copy-start | bytes 49156
  85.0 4.0 %copy-start.6 = (s32[128]{0:T(128)S(1)}, s32[128]{0:T(128)}, u32[]{:S(2)}) copy-start(s32[128]{0:T(128)} %param.21) | copy-start | bytes 1540
  85.0 4.3 %copy-start.2 = (bf16[2048,16]{0,1:T(8,128)(2,1)S(1)}, bf16[2048,16]{0,1:T(8,128)(2,1)}, u32[]{:S(2)}) copy-start(bf16[2048,16]{0,1:T(8,128)(2,1)} %param.20) | copy-start | bytes 196612
  85.0 4.6 %copy-start.4 = (s32[128,2]{0,1:T(2,128)S(1)}, s32[128,2]{0,1:T(2,128)}, u32[]{:S(2)}) copy-start(s32[128,2]{0,1:T(2,128)} %param.22) | copy-start | bytes 3076
  85.8 60.7 %collective-permute-start = (bf16[15,1024]{1,0:T(8,128)(2,1)S(1)}, bf16[15,1024]{1,0:T(8,128)(2,1)S(1)}, u32[]{:S(2)}, u32[]{:S(2)}) collective-permute-start(bf16[15,1024]{1,0:T(8,128)(2,1)S(1)} %slice.136), channel_id=1, source_target_pairs={{0,1},{1,2},{2,3},{3,4},{4,5},{5,6},{6,7},{7,8},{8,9},{9,10},{10,1... | collective-permute-start | bytes 92168 | tf_op jit(solution)/shard_map/ppermute | solution.py:13
  139.4 31.4 %all-to-all-start.1 = ((bf16[16,1024,32]{1,2,0:T(8,128)(2,1)}), bf16[16,1024,32]{1,2,0:T(8,128)(2,1)S(1)}, u32[]{:S(2)}, u32[]{:S(2)}) async-start(bf16[16,1024,32]{1,2,0:T(8,128)(2,1)} %fusion.28), calls=%async_computation.2 | async-start | bytes 2097152 | tf_op jit(solution)/shard_map/all_to_all | solution.py:140
  148.0 1.0 copy-start.9
  149.0 0.7 copy-start.5
  149.0 2.2 %copy-start.7 = (bf16[1024,2048]{1,0:T(8,128)(2,1)S(1)}, bf16[1024,2048]{1,0:T(8,128)(2,1)}, u32[]{:S(2)}) copy-start(bf16[1024,2048]{1,0:T(8,128)(2,1)} %param.16) | copy-start | bytes 12582916
Sparse Core Ops, SparseCore 0:
  85.1 30.8 reduce-scatter.1
